TPU v7x, 32 devices: a whole 2x2x4 slice. The times are simulated.
32 devices in a mesh: fs: 8 (over z, x), tp: 4 (over y, core).
Axes of the slice: x: 2, y: 2, z: 4, core: 2. Of those that a mesh axis runs over, the one named last changes fastest.
Arguments:
- tokens: bfloat16 [2048, 2048], P('fs', 'tp'), may hold values from -6 to 6
- grad_out: bfloat16 [2048, 2048], P('fs', 'tp'), may hold values from -6 to 6
- up_weight: bfloat16 [2048, 4096], P('fs', 'tp'), may hold values from -0.125 to 0.125
- down_weight: bfloat16 [4096, 2048], P('tp', 'fs'), may hold values from -0.09375 to 0.09375
Outputs:
- input_grad: bfloat16 [2048, 2048], P('fs', 'tp')
- up_grad: float32 [2048, 4096], P('fs', 'tp')
- down_grad: float32 [4096, 2048], P('tp', 'fs')
- up_norms: float32 [2048], P('fs')
- down_norms: float32 [4096], P('tp')
All inputs are finite; a program needn't handle non-finite values.
Results may differ from a plain program's by a relative error of at most 0.015.
Values may be sent and summed in bfloat16 or wider, within the bound.
A program may use at most 64 MiB of HBM per device.

v0:
```python
import jax
import jax.numpy as jnp
from jax import lax
from jax.sharding import PartitionSpec as P


def on_device(tokens, grad_out, up_weight, down_weight):
    rows, cotan = (
        lax.all_gather(tokens, "tp", axis=1, tiled=True),
        lax.all_gather(grad_out, "tp", axis=1, tiled=True),
    )
    up_local = lax.all_gather(up_weight, "fs", axis=0, tiled=True)
    dact = lax.dot_general(
        cotan,
        lax.all_gather(down_weight, "fs", axis=1, tiled=True),
        (((1,), (1,)), ((), ())),
        preferred_element_type=jnp.float32,
    )
    pre = jnp.dot(rows, up_local, preferred_element_type=jnp.float32)
    relued = jnp.maximum(pre, 0.0)
    act = (relued * relued).astype(jnp.bfloat16)
    dpre = (dact * 2.0 * relued).astype(jnp.bfloat16)
    partial_sum = lax.dot_general(
        dpre, up_local, (((1,), (1,)), ((), ())), preferred_element_type=jnp.float32
    )
    rounded = lax.optimization_barrier(partial_sum.astype(jnp.bfloat16))
    input_grad = lax.psum_scatter(
        rounded.astype(jnp.float32).astype(jnp.bfloat16), "tp", scatter_dimension=1, tiled=True
    )
    cols = rows
    up_shard = lax.psum_scatter(
        lax.dot_general(
            cols, dpre, (((0,), (0,)), ((), ())), preferred_element_type=jnp.float32
        ).astype(jnp.bfloat16),
        "fs",
        scatter_dimension=0,
        tiled=True,
    ).astype(jnp.float32)
    cols = cotan
    down_flip = lax.psum_scatter(
        lax.dot_general(
            cols, act, (((0,), (0,)), ((), ())), preferred_element_type=jnp.float32
        ).astype(jnp.bfloat16),
        "fs",
        scatter_dimension=0,
        tiled=True,
    ).astype(jnp.float32)
    down_grad = down_flip.T
    up_norms = lax.psum(jnp.sum(up_shard * up_shard, axis=1), "tp")
    down_norms = lax.psum(jnp.sum(down_grad * down_grad, axis=1), "fs")
    return (input_grad, up_shard, down_grad, up_norms, down_norms)


def solution(mesh):
    return jax.shard_map(
        on_device,
        mesh=mesh,
        in_specs=(P("fs", "tp"), P("fs", "tp"), P("fs", "tp"), P("tp", "fs")),
        out_specs=(P("fs", "tp"), P("fs", "tp"), P("tp", "fs"), P("fs"), P("tp")),
        check_vma=False,
    )
```

profile of v0, /device:TPU:0, one launch (start us, length us, event | category | flops | bytes accessed | tf_op | source)
XLA Modules:
  0.0 419.1 jit_solution(4892946634751360285)
XLA Ops:
  7.2 0.0 all-gather.9.cloned.1.call-start
  7.2 0.7 all-gather.9.cloned.1.call-update
  7.9 0.0 all-gather.11.cloned.1.call-start
  7.9 0.7 all-gather.11.cloned.1.call-update
  8.6 0.0 all-gather.5.cloned.1.call-start
  8.7 0.7 all-gather.5.cloned.1.call-update
  9.4 0.0 all-gather.7.cloned.1.call-start
  9.4 0.5 all-gather.7.cloned.1.call-update
  10.0 0.0 reduce-scatter.6.cloned.1.call-start
  10.0 19.0 %all-gather.9.cloned.1.call-done = bf16[256,2048]{1,0:T(8,128)(2,1)} async-done(((bf16[256,512]{1,0:T(8,128)(2,1)}), bf16[256,2048]{1,0:T(8,128)(2,1)}) %all-gather.9.cloned.1.call-update) | async-done | bytes 1048592 | tf_op jit(solution)/shard_map/all_gather | solution.py:9
  29.0 74.9 %all-gather.11.cloned.1.call-done = bf16[2048,1024]{1,0:T(8,128)(2,1)} async-done(((bf16[256,1024]{1,0:T(8,128)(2,1)}), bf16[2048,1024]{1,0:T(8,128)(2,1)}) %all-gather.11.cloned.1.call-update) | async-done | bytes 4194320 | tf_op jit(solution)/shard_map/all_gather | solution.py:12
  103.9 3.8 convolution_maximum_fusion
  107.7 13.1 %all-gather.5.cloned.1.call-done = bf16[256,2048]{1,0:T(8,128)(2,1)} async-done(((bf16[256,512]{1,0:T(8,128)(2,1)}), bf16[256,2048]{1,0:T(8,128)(2,1)}) %all-gather.5.cloned.1.call-update) | async-done | bytes 1048592 | tf_op jit(solution)/shard_map/all_gather | solution.py:10
  120.8 76.6 %all-gather.7.cloned.1.call-done = bf16[1024,2048]{1,0:T(8,128)(2,1)} async-done(((bf16[1024,256]{1,0:T(8,128)(2,1)}), bf16[1024,2048]{1,0:T(8,128)(2,1)}) %all-gather.7.cloned.1.call-update) | async-done | bytes 4194320 | tf_op jit(solution)/shard_map/all_gather | solution.py:15
  197.3 3.8 fusion.1
  201.1 0.0 copy-start
  201.1 4.6 %convert_bitcast_fusion.1 = bf16[2048,1024]{0,1:T(8,128)(2,1)} fusion(bf16[256,1024]{1,0:T(8,128)(2,1)S(1)} %fusion.1, bf16[256,2048]{1,0:T(8,128)(2,1)} %all-gather.9.cloned.1.call-done), kind=kOutput, calls=%fused_computation.1 | convolution fusion | flops 1075838976 | bytes 5767168 | tf_op jit(solution)/shard_map/dot_general | solution.py:32
  205.7 0.0 reduce-scatter.6.cloned.1.call-update
  205.8 0.0 reduce-scatter.8.cloned.1.call-start
  205.8 3.3 convert_bitcast_fusion
  209.1 0.0 reduce-scatter.8.cloned.1.call-update
  209.1 0.0 reduce-scatter.4.cloned.1.call-start
  209.1 4.6 %convolution_convert_fusion = bf16[256,2048]{1,0:T(8,128)(2,1)} fusion(bf16[256,1024]{1,0:T(8,128)(2,1)S(1)} %fusion.1, bf16[2048,1024]{1,0:T(8,128)(2,1)} %all-gather.11.cloned.1.call-done), kind=kOutput, calls=%fused_computation.2 | convolution fusion | flops 1074266112 | bytes 5767168 | tf_op jit(solution)/shard_map/dot_general | solution.py:23
  213.7 0.0 reduce-scatter.4.cloned.1.call-update
  213.7 79.1 %reduce-scatter.6.cloned.1.call-done = bf16[256,1024]{0,1:T(8,128)(2,1)} async-done(((bf16[2048,1024]{0,1:T(8,128)(2,1)}), bf16[256,1024]{0,1:T(8,128)(2,1)}) %reduce-scatter.6.cloned.1.call-update) | async-done | bytes 524304 | tf_op jit(solution)/shard_map/reduce_scatter | solution.py:31
  292.8 2.2 copy.9
  295.1 1.2 multiply_reduce_fusion.1
  296.3 6.7 %psum.14 = f32[256]{0:T(256)} all-reduce(f32[256]{0:T(256)S(1)} %multiply_reduce_fusion.1), channel_id=1, replica_groups=mesh['fs'=8,'tp'=4] {'tp'}, use_global_device_ids=true, to_apply=%region_4.0 | all-reduce | flops 256 | bytes 2048 | tf_op jit(solution)/shard_map/psum | solution.py:49
  303.0 81.7 %reduce-scatter.8.cloned.1.call-done = bf16[256,1024]{0,1:T(8,128)(2,1)} async-done(((bf16[2048,1024]{0,1:T(8,128)(2,1)}), bf16[256,1024]{0,1:T(8,128)(2,1)}) %reduce-scatter.8.cloned.1.call-update) | async-done | bytes 524304 | tf_op jit(solution)/shard_map/reduce_scatter | solution.py:40
  384.7 2.1 multiply_reduce_fusion
  386.8 20.6 %psum.15 = f32[1024]{0:T(1024)} all-reduce(f32[1024]{0:T(1024)S(1)} %get-tuple-element.10), channel_id=1, replica_groups=mesh['fs'=8,'tp'=4] {'fs'}, use_global_device_ids=true, to_apply=%region_6.0 | all-reduce | flops 1024 | bytes 8192 | tf_op jit(solution)/shard_map/psum | solution.py:50
  407.4 4.8 %reduce-scatter.4.cloned.1.call-done = bf16[256,512]{1,0:T(8,128)(2,1)} async-done(((bf16[256,2048]{1,0:T(8,128)(2,1)}), bf16[256,512]{1,0:T(8,128)(2,1)}) %reduce-scatter.4.cloned.1.call-update) | async-done | bytes 262160 | tf_op jit(solution)/shard_map/reduce_scatter | solution.py:27
  (1 shorter events, 0.0 us)
Async XLA Ops:
  7.2 21.8 %all-gather.9.cloned.1.call-start = ((), (), s32[]{:S(2)}) async-start(), calls=%async_computation.5 | async-start | bytes 1310720 | tf_op jit(solution)/shard_map/all_gather | solution.py:9
  7.9 96.0 %all-gather.11.cloned.1.call-start = ((), (), s32[]{:S(2)}) async-start(), calls=%async_computation.6 | async-start | bytes 4718592 | tf_op jit(solution)/shard_map/all_gather | solution.py:12
  8.6 112.1 %all-gather.5.cloned.1.call-start = ((), (), s32[]{:S(2)}) async-start(), calls=%async_computation.3 | async-start | bytes 1310720 | tf_op jit(solution)/shard_map/all_gather | solution.py:10
  9.4 188.0 %all-gather.7.cloned.1.call-start = ((), (), s32[]{:S(2)}) async-start(), calls=%async_computation.4 | async-start | bytes 4718592 | tf_op jit(solution)/shard_map/all_gather | solution.py:15
  10.0 282.9 %reduce-scatter.6.cloned.1.call-start = ((), (), s32[]{:S(2)}) async-start(), calls=%async_computation.8 | async-start | bytes 4718592 | tf_op jit(solution)/shard_map/reduce_scatter | solution.py:31
  201.1 4.7 %copy-start = (bf16[256,2048]{1,0:T(8,128)(2,1)S(1)}, bf16[256,2048]{1,0:T(8,128)(2,1)}, u32[]{:S(2)}) copy-start(bf16[256,2048]{1,0:T(8,128)(2,1)} %all-gather.5.cloned.1.call-done) | copy-start | bytes 3145732
  205.8 179.0 %reduce-scatter.8.cloned.1.call-start = ((), (), s32[]{:S(2)}) async-start(), calls=%async_computation.9 | async-start | bytes 4718592 | tf_op jit(solution)/shard_map/reduce_scatter | solution.py:40
  209.1 203.2 %reduce-scatter.4.cloned.1.call-start = ((), (), s32[]{:S(2)}) async-start(), calls=%async_computation.7 | async-start | bytes 1310720 | tf_op jit(solution)/shard_map/reduce_scatter | solution.py:27
Sparse Core Ops, SparseCore 0:
  9.5 19.4 all-gather.8
  31.1 72.7 all-gather.10
  105.5 15.2 all-gather.4
  122.7 74.6 all-gather.6
  205.9 86.9 reduce-scatter.5
  296.3 88.3 reduce-scatter.7
  387.8 24.4 reduce-scatter.3
where the time goes:
time: 419 us
  waiting for transfers between devices  352 us (84%)
  blocking collectives  27.4 us (7%)
  matrix products  20 us (5%)
  between operations  14.2 us (3%)
    reduce_scatter x1, waiting for transfers between devices, on_device(): lax.psum_scatter(lax.dot_general(cols, act, (((0,), (0,)), ((), ())), pre...  81.7 us
    reduce_scatter x1, waiting for transfers between devices, on_device(): lax.psum_scatter(lax.dot_general(cols, dpre, (((0,), (0,)), ((), ())), pr...  79.1 us
    all_gather x1, waiting for transfers between devices, on_device(): lax.all_gather(down_weight, 'fs', axis=1, tiled=True)  76.6 us
    all_gather x1, waiting for transfers between devices, on_device(): up_local = lax.all_gather(up_weight, 'fs', axis=0, tiled=True)  74.9 us
    psum x1, blocking collectives, on_device(): down_norms = lax.psum(jnp.sum(down_grad * down_grad, axis=1), 'fs')  20.6 us
    all_gather x1, waiting for transfers between devices, on_device(): lax.all_gather(tokens, 'tp', axis=1, tiled=True)  19 us
    all_gather x1, waiting for transfers between devices, on_device(): lax.all_gather(grad_out, 'tp', axis=1, tiled=True)  13.1 us
  transfers between devices with their start and end apart: 7, of which 7 were waited for; matrix products, arithmetic and copies ran while one was open for 4% of the time, Pallas kernels for 0%

commit v1 on v0

--- a/solution.py
+++ b/solution.py
@@ -9,7 +9,20 @@
         lax.all_gather(tokens, "tp", axis=1, tiled=True),
         lax.all_gather(grad_out, "tp", axis=1, tiled=True),
     )
-    up_local = lax.all_gather(up_weight, "fs", axis=0, tiled=True)
+
+    def list_sector(vals):
+        total_devices = lax.axis_size("fs")
+        found = [(no, (no + 1) % total_devices) for no in range(total_devices)]
+
+        def chunk_return_all(v1):
+            if len(v1) == total_devices:
+                return v1
+            return chunk_return_all([lax.ppermute(v1[0], "fs", found), *v1])
+
+        block_next = jnp.concatenate(chunk_return_all([vals]), axis=0)
+        return jnp.roll(block_next, (lax.axis_index("fs") + 1) * vals.shape[0], 0)
+
+    up_local = list_sector(up_weight)
     dact = lax.dot_general(
         cotan,
         lax.all_gather(down_weight, "fs", axis=1, tiled=True),

time: 419 us -> 393 us (0.938)
  waiting for transfers between devices: 352 us -> 304 us
  local copies, waits for them, and re-layouts: 2.22 us -> 19.7 us
    ppermute x0 -> x7, waiting for transfers between devices: none -> 143 us  [chunk_return_all(): return chunk_return_all([lax.ppermute(v1[0], 'fs', found), *v1])]
    all_gather x1, waiting for transfers between devices: 76.6 us -> 0.02 us  [on_device(): lax.all_gather(down_weight, 'fs', axis=1, tiled=True)]
    all_gather x1 -> x0, waiting for transfers between devices: 74.9 us -> none  [on_device(): up_local = lax.all_gather(up_weight, 'fs', axis=0, tiled=True)]
    all_gather x1, waiting for transfers between devices: 19 us -> 0.01 us  [on_device(): lax.all_gather(tokens, 'tp', axis=1, tiled=True)]
    unnamed x3 -> x20, local copies, waits for them, and re-layouts: 2.22 us -> 18.8 us
    all_gather x1, waiting for transfers between devices: 13.1 us -> 0.02 us  [on_device(): lax.all_gather(grad_out, 'tp', axis=1, tiled=True)]
    reduce_scatter x1, waiting for transfers between devices: 4.82 us -> 17.3 us  [on_device(): lax.psum_scatter(rounded.astype(jnp.float32).astype(jnp.bfloat16), 'tp',...]
    reduce_scatter x1, waiting for transfers between devices: 79.1 us -> 68.6 us  [on_device(): lax.psum_scatter(lax.dot_general(cols, dpre, (((0,), (0,)), ((), ())), pr...]
  transfers between devices with their start and end apart: 7 -> 13, of which waited for: 7 -> 10; matrix products, arithmetic and copies ran while one was open for 4% -> 11% of each run, Pallas kernels for 0% -> 0%
where the time goes in v1:
time: 393 us
  waiting for transfers between devices  304 us (77%)
  blocking collectives  28 us (7%)
  matrix products  20.7 us (5%)
  local copies, waits for them, and re-layouts  19.7 us (5%)
  between operations  14.2 us (4%)
    ppermute x7, waiting for transfers between devices, chunk_return_all(): return chunk_return_all([lax.ppermute(v1[0], 'fs', found), *v1])  143 us
    reduce_scatter x1, waiting for transfers between devices, on_device(): lax.psum_scatter(lax.dot_general(cols, act, (((0,), (0,)), ((), ())), pre...  72.2 us
    reduce_scatter x1, waiting for transfers between devices, on_device(): lax.psum_scatter(lax.dot_general(cols, dpre, (((0,), (0,)), ((), ())), pr...  68.6 us
    psum x1, blocking collectives, on_device(): down_norms = lax.psum(jnp.sum(down_grad * down_grad, axis=1), 'fs')  21.3 us
    unnamed x20, local copies, waits for them, and re-layouts  18.8 us
    reduce_scatter x1, waiting for transfers between devices, on_device(): lax.psum_scatter(rounded.astype(jnp.float32).astype(jnp.bfloat16), 'tp',...  17.3 us
  transfers between devices with their start and end apart: 13, of which 10 were waited for; matrix products, arithmetic and copies ran while one was open for 11% of the time, Pallas kernels for 0%

profile of v1, /device:TPU:0, one launch (start us, length us, event | category | flops | bytes accessed | tf_op | source)
XLA Modules:
  0.0 392.7 jit_solution(16833318764412643)
XLA Ops:
  9.4 3.0 collective-permute-start
  12.5 15.2 %collective-permute-done = bf16[256,1024]{1,0:T(8,128)(2,1)S(1)} collective-permute-done((bf16[256,1024]{1,0:T(8,128)(2,1)}, bf16[256,1024]{1,0:T(8,128)(2,1)S(1)}, u32[]{:S(2)}, u32[]{:S(2)}) %collective-permute-start) | collective-permute-done | bytes 524320 | tf_op jit(solution)/shard_map/ppermute | solution.py:20
  27.6 15.8 %collective-permute-done.1 = bf16[256,1024]{1,0:T(8,128)(2,1)S(1)} collective-permute-done((bf16[256,1024]{1,0:T(8,128)(2,1)S(1)}, bf16[256,1024]{1,0:T(8,128)(2,1)S(1)}, u32[]{:S(2)}, u32[]{:S(2)}) %collective-permute-start.1) | collective-permute-done | bytes 524320 | tf_op jit(solution)/shard_map/ppermute | solution.py:20
  43.4 14.9 %collective-permute-done.2 = bf16[256,1024]{1,0:T(8,128)(2,1)S(1)} collective-permute-done((bf16[256,1024]{1,0:T(8,128)(2,1)S(1)}, bf16[256,1024]{1,0:T(8,128)(2,1)S(1)}, u32[]{:S(2)}, u32[]{:S(2)}) %collective-permute-start.2) | collective-permute-done | bytes 524320 | tf_op jit(solution)/shard_map/ppermute | solution.py:20
  58.3 26.4 %collective-permute-done.3 = bf16[256,1024]{1,0:T(8,128)(2,1)S(1)} collective-permute-done((bf16[256,1024]{1,0:T(8,128)(2,1)S(1)}, bf16[256,1024]{1,0:T(8,128)(2,1)S(1)}, u32[]{:S(2)}, u32[]{:S(2)}) %collective-permute-start.3) | collective-permute-done | bytes 524320 | tf_op jit(solution)/shard_map/ppermute | solution.py:20
  84.8 15.8 %collective-permute-done.4 = bf16[256,1024]{1,0:T(8,128)(2,1)S(1)} collective-permute-done((bf16[256,1024]{1,0:T(8,128)(2,1)S(1)}, bf16[256,1024]{1,0:T(8,128)(2,1)S(1)}, u32[]{:S(2)}, u32[]{:S(2)}) %collective-permute-start.4) | collective-permute-done | bytes 524320 | tf_op jit(solution)/shard_map/ppermute | solution.py:20
  100.6 27.6 %collective-permute-done.5 = bf16[256,1024]{1,0:T(8,128)(2,1)} collective-permute-done((bf16[256,1024]{1,0:T(8,128)(2,1)S(1)}, bf16[256,1024]{1,0:T(8,128)(2,1)}, u32[]{:S(2)}, u32[]{:S(2)}) %collective-permute-start.5) | collective-permute-done | bytes 524320 | tf_op jit(solution)/shard_map/ppermute | solution.py:20
  128.2 27.5 %collective-permute-done.6 = bf16[256,1024]{1,0:T(8,128)(2,1)} collective-permute-done((bf16[256,1024]{1,0:T(8,128)(2,1)}, bf16[256,1024]{1,0:T(8,128)(2,1)}, u32[]{:S(2)}, u32[]{:S(2)}) %collective-permute-start.6) | collective-permute-done | bytes 524320 | tf_op jit(solution)/shard_map/ppermute | solution.py:20
  155.7 1.9 constant_dynamic-update-slice_fusion.15
  157.6 1.9 constant_dynamic-update-slice_fusion.14
  159.4 0.8 constant_dynamic-update-slice_fusion.13
  161.1 0.8 constant_dynamic-update-slice_fusion.11
  162.0 0.8 constant_dynamic-update-slice_fusion.10
  164.4 1.9 constant_dynamic-update-slice_fusion.7
  166.3 1.9 constant_dynamic-update-slice_fusion.6
  168.2 0.8 constant_dynamic-update-slice_fusion.5
  169.9 0.8 constant_dynamic-update-slice_fusion.3
  170.7 0.8 constant_dynamic-update-slice_fusion.2
  172.3 0.9 constant_dynamic-update-slice_fusion
  173.2 3.8 fusion.10
  177.0 4.5 %convert_bitcast_fusion = bf16[2048,1024]{0,1:T(8,128)(2,1)} fusion(bf16[256,2048]{1,0:T(8,128)(2,1)} %all-gather.4.cloned.1.call-done, f32[256,1024]{1,0:T(8,128)S(1)} %fusion.10), kind=kOutput, calls=%fused_computation | convolution fusion | flops 1076363264 | bytes 6291456 | tf_op jit(solution)/shard_map/dot_general | solution.py:54
  181.7 3.5 fusion.14
  185.2 4.5 %convert_bitcast_fusion.1 = bf16[2048,1024]{0,1:T(8,128)(2,1)} fusion(bf16[256,1024]{1,0:T(8,128)(2,1)S(1)} %fusion.14, bf16[256,2048]{1,0:T(8,128)(2,1)} %all-gather.8.cloned.1.call-done), kind=kOutput, calls=%fused_computation.1 | convolution fusion | flops 1075838976 | bytes 5767168 | tf_op jit(solution)/shard_map/dot_general | solution.py:45
  189.7 4.5 %fusion.4 = bf16[256,2048]{1,0:T(8,128)(2,1)} fusion(bf16[256,1024]{1,0:T(8,128)(2,1)S(1)} %fusion.14, bf16[4096,1024]{1,0:T(8,128)(2,1)} %constant_dynamic-update-slice_fusion, s32[]{:T(128)S(6)} %select_n.14), kind=kOutput, calls=%fused_computation.6 | convolution fusion | flops 1074266112 | bytes 5767172 | tf_op jit(solution)/shard_map/dot_general | solution.py:36
  194.2 72.2 %reduce-scatter.8.cloned.1.call-done = bf16[256,1024]{0,1:T(8,128)(2,1)} async-done(((bf16[2048,1024]{0,1:T(8,128)(2,1)}), bf16[256,1024]{0,1:T(8,128)(2,1)}) %reduce-scatter.8.cloned.1.call-update) | async-done | bytes 524304 | tf_op jit(solution)/shard_map/reduce_scatter | solution.py:53
  266.5 2.1 multiply_reduce_fusion
  268.6 21.3 %psum.15 = f32[1024]{0:T(1024)} all-reduce(f32[1024]{0:T(1024)S(1)} %get-tuple-element.10), channel_id=1, replica_groups=mesh['fs'=8,'tp'=4] {'fs'}, use_global_device_ids=true, to_apply=%region_6.7 | all-reduce | flops 1024 | bytes 8192 | tf_op jit(solution)/shard_map/psum | solution.py:63
  289.8 68.6 %reduce-scatter.6.cloned.1.call-done = bf16[256,1024]{0,1:T(8,128)(2,1)} async-done(((bf16[2048,1024]{0,1:T(8,128)(2,1)}), bf16[256,1024]{0,1:T(8,128)(2,1)}) %reduce-scatter.6.cloned.1.call-update) | async-done | bytes 524304 | tf_op jit(solution)/shard_map/reduce_scatter | solution.py:44
  358.4 2.2 copy.10
  360.7 1.2 multiply_reduce_fusion.1
  361.9 6.7 %psum.14 = f32[256]{0:T(256)} all-reduce(f32[256]{0:T(256)S(1)} %multiply_reduce_fusion.1), channel_id=1, replica_groups=mesh['fs'=8,'tp'=4] {'tp'}, use_global_device_ids=true, to_apply=%region_4.5 | all-reduce | flops 256 | bytes 2048 | tf_op jit(solution)/shard_map/psum | solution.py:62
  368.6 17.3 %reduce-scatter.4.cloned.1.call-done = bf16[256,512]{1,0:T(8,128)(2,1)} async-done(((bf16[256,2048]{1,0:T(8,128)(2,1)}), bf16[256,512]{1,0:T(8,128)(2,1)}) %reduce-scatter.4.cloned.1.call-update) | async-done | bytes 262160 | tf_op jit(solution)/shard_map/reduce_scatter | solution.py:40
  (30 shorter events, 6.5 us)
Async XLA Ops:
  7.2 156.5 %copy-start = (bf16[256,1024]{1,0:T(8,128)(2,1)S(1)}, bf16[256,1024]{1,0:T(8,128)(2,1)}, u32[]{:S(2)}) copy-start(bf16[256,1024]{1,0:T(8,128)(2,1)} %param.6) | copy-start | bytes 1572868
  7.2 166.0 %all-gather.8.cloned.1.call-start = ((), (), s32[]{:S(2)}) async-start(), calls=%async_computation.5 | async-start | bytes 1310720 | tf_op jit(solution)/shard_map/all_gather | solution.py:9
  7.9 169.1 %all-gather.4.cloned.1.call-start = ((), (), s32[]{:S(2)}) async-start(), calls=%async_computation.3 | async-start | bytes 1310720 | tf_op jit(solution)/shard_map/all_gather | solution.py:10
  8.7 173.0 %all-gather.6.cloned.1.call-start = ((), (), s32[]{:S(2)}) async-start(), calls=%async_computation.4 | async-start | bytes 4718592 | tf_op jit(solution)/shard_map/all_gather | solution.py:28
  9.4 257.1 %reduce-scatter.8.cloned.1.call-start = ((), (), s32[]{:S(2)}) async-start(), calls=%async_computation.8 | async-start | bytes 4718592 | tf_op jit(solution)/shard_map/reduce_scatter | solution.py:53
  9.4 18.2 %collective-permute-start = (bf16[256,1024]{1,0:T(8,128)(2,1)}, bf16[256,1024]{1,0:T(8,128)(2,1)S(1)}, u32[]{:S(2)}, u32[]{:S(2)}) collective-permute-start(bf16[256,1024]{1,0:T(8,128)(2,1)} %param.6), channel_id=1, source_target_pairs={{0,4},{4,8},{8,12},{12,16},{16,20},{20,24},{24,28},{28,0},{1,5},{5... | collective-permute-start | bytes 1572872 | tf_op jit(solution)/shard_map/ppermute | solution.py:20
  27.6 15.8 %collective-permute-start.1 = (bf16[256,1024]{1,0:T(8,128)(2,1)S(1)}, bf16[256,1024]{1,0:T(8,128)(2,1)S(1)}, u32[]{:S(2)}, u32[]{:S(2)}) collective-permute-start(bf16[256,1024]{1,0:T(8,128)(2,1)S(1)} %collective-permute-done), channel_id=1, source_target_pairs={{0,4},{4,8},{8,12},{12,16},{16,20},{20,24},{24,28},{28,0},{1,5},{5... | collective-permute-start | bytes 1572872 | tf_op jit(solution)/shard_map/ppermute | solution.py:20
  43.4 14.9 %collective-permute-start.2 = (bf16[256,1024]{1,0:T(8,128)(2,1)S(1)}, bf16[256,1024]{1,0:T(8,128)(2,1)S(1)}, u32[]{:S(2)}, u32[]{:S(2)}) collective-permute-start(bf16[256,1024]{1,0:T(8,128)(2,1)S(1)} %collective-permute-done.1), channel_id=1, source_target_pairs={{0,4},{4,8},{8,12},{12,16},{16,20},{20,24},{24,28},{28,0},{1,5},{5... | collective-permute-start | bytes 1572872 | tf_op jit(solution)/shard_map/ppermute | solution.py:20
  58.3 26.4 %collective-permute-start.3 = (bf16[256,1024]{1,0:T(8,128)(2,1)S(1)}, bf16[256,1024]{1,0:T(8,128)(2,1)S(1)}, u32[]{:S(2)}, u32[]{:S(2)}) collective-permute-start(bf16[256,1024]{1,0:T(8,128)(2,1)S(1)} %collective-permute-done.2), channel_id=1, source_target_pairs={{0,4},{4,8},{8,12},{12,16},{16,20},{20,24},{24,28},{28,0},{1,5},{5... | collective-permute-start | bytes 1572872 | tf_op jit(solution)/shard_map/ppermute | solution.py:20
  84.8 15.8 %collective-permute-start.4 = (bf16[256,1024]{1,0:T(8,128)(2,1)S(1)}, bf16[256,1024]{1,0:T(8,128)(2,1)S(1)}, u32[]{:S(2)}, u32[]{:S(2)}) collective-permute-start(bf16[256,1024]{1,0:T(8,128)(2,1)S(1)} %collective-permute-done.3), channel_id=1, source_target_pairs={{0,4},{4,8},{8,12},{12,16},{16,20},{20,24},{24,28},{28,0},{1,5},{5... | collective-permute-start | bytes 1572872 | tf_op jit(solution)/shard_map/ppermute | solution.py:20
  100.6 27.6 %collective-permute-start.5 = (bf16[256,1024]{1,0:T(8,128)(2,1)S(1)}, bf16[256,1024]{1,0:T(8,128)(2,1)}, u32[]{:S(2)}, u32[]{:S(2)}) collective-permute-start(bf16[256,1024]{1,0:T(8,128)(2,1)S(1)} %collective-permute-done.4), channel_id=1, source_target_pairs={{0,4},{4,8},{8,12},{12,16},{16,20},{20,24},{24,28},{28,0},{1,5},{5... | collective-permute-start | bytes 1572872 | tf_op jit(solution)/shard_map/ppermute | solution.py:20
  128.2 27.5 %collective-permute-start.6 = (bf16[256,1024]{1,0:T(8,128)(2,1)}, bf16[256,1024]{1,0:T(8,128)(2,1)}, u32[]{:S(2)}, u32[]{:S(2)}) collective-permute-start(bf16[256,1024]{1,0:T(8,128)(2,1)} %collective-permute-done.5), channel_id=1, source_target_pairs={{0,4},{4,8},{8,12},{12,16},{16,20},{20,24},{24,28},{28,0},{1,5},{5... | collective-permute-start | bytes 1572872 | tf_op jit(solution)/shard_map/ppermute | solution.py:20
  177.0 4.7 %copy-start.1 = (bf16[256,2048]{1,0:T(8,128)(2,1)S(1)}, bf16[256,2048]{1,0:T(8,128)(2,1)}, u32[]{:S(2)}) copy-start(bf16[256,2048]{1,0:T(8,128)(2,1)} %all-gather.4.cloned.1.call-done) | copy-start | bytes 3145732
  181.6 176.9 %reduce-scatter.6.cloned.1.call-start = ((), (), s32[]{:S(2)}) async-start(), calls=%async_computation.7 | async-start | bytes 4718592 | tf_op jit(solution)/shard_map/reduce_scatter | solution.py:44
  189.7 196.2 %reduce-scatter.4.cloned.1.call-start = ((), (), s32[]{:S(2)}) async-start(), calls=%async_computation.6 | async-start | bytes 1310720 | tf_op jit(solution)/shard_map/reduce_scatter | solution.py:40
Sparse Core Ops, SparseCore 0:
  9.5 19.4 all-gather.7
  30.6 16.6 all-gather.3
  49.3 101.5 all-gather.5
  181.7 84.6 reduce-scatter.7
  269.9 88.4 reduce-scatter.5
  361.4 24.4 reduce-scatter.3
